TPU v7x, 32 devices: a whole 2x2x4 slice. The times are simulated.
32 devices in a mesh: rep: 2 (over x), fs: 8 (over z, y), tp: 2 (over core).
Axes of the slice: x: 2, y: 2, z: 4, core: 2. Of those that a mesh axis runs over, the one named last changes fastest.
Arguments:
- inputs: bfloat16 [8192, 2048], P(('rep', 'fs')), may hold values from -6 to 6
- gain: float32 [2048], replicated, may hold values from 0.1 to 1.9
- gate_weight: bfloat16 [2048, 3072], P('fs', 'tp'), may hold values from -0.125 to 0.125
- up_weight: bfloat16 [2048, 3072], P('fs', 'tp'), may hold values from -0.125 to 0.125
- down_weight: bfloat16 [2048, 3072], P('fs', 'tp'), may hold values from -0.109375 to 0.109375
- cotangent: bfloat16 [8192, 2048], P(('rep', 'fs')), may hold values from -6 to 6
Outputs:
- input_gradient: bfloat16 [8192, 2048], P(('rep', 'fs'))
- gain_gradient: float32 [2048], replicated
- d_down: float32 [2048, 3072], P('fs', 'tp')
All inputs are finite; a program needn't handle non-finite values.
Results may differ from a plain program's by a relative error of at most 0.014.
Values may be sent and summed in bfloat16 or wider, within the bound.
A program may use at most 128 MiB of HBM per device.

v0:
```python
import jax
import jax.numpy as jnp
from jax import lax
from jax.sharding import PartitionSpec as P

EPS = 1e-06


def local(inputs, gain, gate_weight, up_weight, down_weight, cotangent):
    single_precision = inputs.astype(jnp.float32)
    reciprocal_root_mean = lax.rsqrt(
        jnp.mean(single_precision * single_precision, axis=-1, keepdims=True) + EPS
    )
    unit_input = single_precision * reciprocal_root_mean
    normalized_input = (unit_input * gain).astype(jnp.bfloat16)
    row_count = inputs.shape[0]
    contract_cols = (((1,), (1,)), ((), ()))
    gate_full, up_full, down_full = (
        lax.all_gather(gate_weight, "fs", axis=0, tiled=True),
        lax.all_gather(up_weight, "fs", axis=0, tiled=True),
        lax.all_gather(down_weight, "fs", axis=0, tiled=True),
    )
    gate = jnp.dot(normalized_input, gate_full, preferred_element_type=jnp.float32)
    up_proj = jnp.dot(normalized_input, up_full, preferred_element_type=jnp.float32)
    down_sum = jnp.dot(cotangent, down_full, preferred_element_type=jnp.float32)
    gate_sig = jax.nn.sigmoid(gate)
    active = gate * gate_sig
    hidden = (active * up_proj).astype(jnp.bfloat16)
    d_hidden = 0.5 * down_sum
    d_gate = (d_hidden * up_proj * gate_sig * (1.0 + gate * (1.0 - gate_sig))).astype(jnp.bfloat16)
    d_up = (d_hidden * active).astype(jnp.bfloat16)
    partial_value = lax.dot_general(
        d_gate, gate_full, contract_cols, preferred_element_type=jnp.float32
    ) + lax.dot_general(d_up, up_full, contract_cols, preferred_element_type=jnp.float32)
    summed_units = lax.psum(partial_value.astype(jnp.bfloat16), "tp")
    normalized_gradient = summed_units.astype(jnp.float32)
    gain_gradient = lax.psum(jnp.sum(normalized_gradient * unit_input, axis=0), ("rep", "fs"))
    gain_scaled = gain * normalized_gradient
    mean_correction = jnp.mean(gain_scaled * unit_input, axis=-1, keepdims=True)
    input_gradient = (
        cotangent.astype(jnp.float32)
        + reciprocal_root_mean * (gain_scaled - unit_input * mean_correction)
    ).astype(jnp.bfloat16)
    contract_rows = (((0,), (0,)), ((), ()))
    width = cotangent.shape[1]
    groups_fs = lax.axis_size("fs")
    groups_rep = lax.axis_size("rep")
    sub_rows = width // (groups_fs * groups_rep)
    reordered = (
        cotangent.reshape(row_count, groups_fs, groups_rep, sub_rows)
        .transpose(0, 2, 1, 3)
        .reshape(row_count, width)
    )
    summed = lax.psum_scatter(
        0.5 * lax.dot_general(reordered, hidden, contract_rows, preferred_element_type=jnp.float32),
        ("rep", "fs"),
        scatter_dimension=0,
        tiled=True,
    )
    d_down = lax.all_gather(summed, "rep", axis=0, tiled=True)
    return (input_gradient, gain_gradient, d_down)


def solution(mesh):
    placed = (
        P(("rep", "fs"), None),
        P(),
        P("fs", "tp"),
        P("fs", "tp"),
        P("fs", "tp"),
        P(("rep", "fs"), None),
    )
    return jax.shard_map(
        local,
        mesh=mesh,
        in_specs=placed,
        out_specs=(P(("rep", "fs"), None), P(), P("fs", "tp")),
        check_vma=False,
    )
```

profile of v0, /device:TPU:0, one launch (start us, length us, event | category | flops | bytes accessed | tf_op | source)
XLA Modules:
  0.0 600.7 jit_solution(4841965839708579481)
XLA Ops:
  7.2 0.0 copy-start.1
  7.2 0.0 all-gather.9.cloned.1.call-start
  7.2 0.7 all-gather.9.cloned.1.call-update
  7.9 0.0 all-gather.7.cloned.1.call-start
  8.0 0.7 all-gather.7.cloned.1.call-update
  8.7 0.0 all-gather.5.cloned.1.call-start
  8.7 0.7 all-gather.5.cloned.1.call-update
  9.4 0.0 reduce-scatter.2.cloned.1.call-start
  9.4 0.0 copy-done.1
  9.5 2.5 copy.11
  12.0 0.0 copy-start
  12.0 0.0 copy-start.3
  12.0 3.3 copy.12
  15.2 0.0 copy-done
  15.2 0.5 fusion.9
  15.7 95.9 %all-gather.9.cloned.1.call-done = bf16[2048,1536]{1,0:T(8,128)(2,1)} async-done(((bf16[256,1536]{1,0:T(8,128)(2,1)}), bf16[2048,1536]{1,0:T(8,128)(2,1)}) %all-gather.9.cloned.1.call-update) | async-done | bytes 6291472 | tf_op jit(solution)/shard_map/all_gather | solution.py:19
  111.6 0.0 copy-done.3
  111.6 7.9 %fusion.14 = f32[512,1536]{1,0:T(8,128)} fusion(bf16[2048,1536]{1,0:T(8,128)(2,1)} %all-gather.9.cloned.1.call-done, bf16[512,2048]{1,0:T(8,128)(2,1)S(1)} %copy-done, f32[2048]{0:T(1024)S(1)} %copy-done.3, f32[512]{0:T(512)S(1)} %add_rsqrt_fusion), kind=kOutput, calls=%fused_computation.25 | convolution fusion | flops 3225419776 | bytes 11544576 | tf_op jit(solution)/shard_map/dot_general | solution.py:23
  119.5 91.2 %all-gather.7.cloned.1.call-done = bf16[2048,1536]{1,0:T(8,128)(2,1)} async-done(((bf16[256,1536]{1,0:T(8,128)(2,1)}), bf16[2048,1536]{1,0:T(8,128)(2,1)}) %all-gather.7.cloned.1.call-update) | async-done | bytes 6291472 | tf_op jit(solution)/shard_map/all_gather | solution.py:20
  210.7 0.0 copy-start.2
  210.7 0.0 copy-start.4
  210.7 5.8 fusion.16
  216.5 0.0 copy-start.6
  216.5 1.7 copy-done.6
  218.2 0.0 copy-done.2
  218.2 0.0 copy-done.4
  218.2 6.8 %multiply_bitcast_fusion = f32[2048,1536]{0,1:T(8,128)} fusion(bf16[512,2048]{0,1:T(8,128)(2,1)S(1)} %bitcast.14, f32[512,1536]{1,0:T(8,128)S(1)} %fusion.16, f32[512,1536]{1,0:T(8,128)S(1)} %copy-done.4), kind=kOutput, calls=%fused_computation | convolution fusion | flops 3229089792 | bytes 20971520 | tf_op jit(solution)/shard_map/dot_general | solution.py:55
  225.1 0.0 reduce-scatter.2.cloned.1.call-update
  225.1 0.2 all-reduce.2.cloned.1.call-start
  225.3 84.5 %all-gather.5.cloned.1.call-done = bf16[2048,1536]{1,0:T(8,128)(2,1)} async-done(((bf16[256,1536]{1,0:T(8,128)(2,1)}), bf16[2048,1536]{1,0:T(8,128)(2,1)}) %all-gather.5.cloned.1.call-update) | async-done | bytes 6291472 | tf_op jit(solution)/shard_map/all_gather | solution.py:21
  309.8 0.0 copy-start.5
  309.8 0.0 copy-start.7
  309.8 0.0 slice-start
  309.8 8.6 %convolution_multiply_fusion = f32[512,1536]{1,0:T(8,128)} fusion(bf16[512,2048]{1,0:T(8,128)(2,1)} %param.11, bf16[2048,1536]{1,0:T(8,128)(2,1)} %all-gather.5.cloned.1.call-done), kind=kOutput, calls=%fused_computation.17 | convolution fusion | flops 3222011904 | bytes 11534336 | tf_op jit(solution)/shard_map/dot_general | solution.py:25
  318.4 0.0 copy-done.5
  318.4 0.0 copy-done.7
  318.4 0.0 slice-start.1
  318.4 8.6 %fusion.12 = f32[512,2048]{1,0:T(8,128)S(1)} fusion(bf16[2048,1536]{1,0:T(8,128)(2,1)} %all-gather.9.cloned.1.call-done, f32[512,1536]{1,0:T(8,128)S(1)} %copy-done.5, f32[512,1536]{1,0:T(8,128)} %convolution_multiply_fusion, f32[512,1536]{1,0:T(8,128)S(1)} %copy-done.7), kind=kOutput, calls=%fused_computation.23 | convolution fusion | flops 3229089792 | bytes 19922944 | tf_op jit(solution)/shard_map/dot_general | solution.py:32
  327.0 0.0 slice-done
  327.0 0.0 slice-done.1
  327.1 6.6 %add_convert_fusion = bf16[512,2048]{1,0:T(8,128)(2,1)} fusion(f32[512,2048]{1,0:T(8,128)S(1)} %fusion.12, bf16[2048,1536]{1,0:T(8,128)(2,1)S(1)} %bitcast.16, f32[512,1536]{1,0:T(8,128)} %convolution_multiply_fusion, f32[512,1536]{1,0:T(8,128)S(1)} %copy-done.5), kind=kOutput, calls=%fused_computation.16 | convolution fusion | flops 3228041216 | bytes 18874368 | tf_op jit(solution)/shard_map/dot_general | solution.py:34
  333.7 0.0 all-reduce.2.cloned.1.call-update
  333.7 0.0 all-gather.11.cloned.1.call-start
  333.7 182.3 %reduce-scatter.2.cloned.1.call-done = f32[128,1536]{0,1:T(8,128)} async-done(((f32[2048,1536]{0,1:T(8,128)}), f32[128,1536]{0,1:T(8,128)}) %reduce-scatter.2.cloned.1.call-update) | async-done | bytes 786448 | tf_op jit(solution)/shard_map/reduce_scatter | solution.py:54
  516.0 0.0 all-gather.11.cloned.1.call-update
  516.1 23.6 %all-reduce.2.cloned.1.call-done = bf16[512,2048]{1,0:T(8,128)(2,1)} async-done(((bf16[512,2048]{1,0:T(8,128)(2,1)}), bf16[512,2048]{1,0:T(8,128)(2,1)}) %all-reduce.2.cloned.1.call-update) | async-done | bytes 2097168 | tf_op jit(solution)/shard_map/psum | solution.py:35
  539.6 2.9 fusion.10
  542.5 43.3 %psum.15 = f32[2048]{0:T(1024)} all-reduce(f32[2048]{0:T(1024)S(1)} %get-tuple-element.12), channel_id=1, replica_groups=mesh['rep'=2,'fs'=8,'tp'=2] {'rep','fs'}, use_global_device_ids=true, to_apply=%region_4.0 | all-reduce | flops 2048 | bytes 16384 | tf_op jit(solution)/shard_map/psum | solution.py:37
  585.8 5.0 fusion.6
  590.8 0.0 all-gather.11.cloned.1.call-done
  590.8 3.0 copy.13
  (3 shorter events, 0.0 us)
Async XLA Ops:
  7.2 2.3 copy-start.1
  7.2 104.4 %all-gather.9.cloned.1.call-start = ((), (), s32[]{:S(2)}) async-start(), calls=%async_computation.3 | async-start | bytes 7077888 | tf_op jit(solution)/shard_map/all_gather | solution.py:19
  7.9 202.8 %all-gather.7.cloned.1.call-start = ((), (), s32[]{:S(2)}) async-start(), calls=%async_computation.2 | async-start | bytes 7077888 | tf_op jit(solution)/shard_map/all_gather | solution.py:20
  8.7 301.1 %all-gather.5.cloned.1.call-start = ((), (), s32[]{:S(2)}) async-start(), calls=%async_computation.1 | async-start | bytes 7077888 | tf_op jit(solution)/shard_map/all_gather | solution.py:21
  9.4 506.6 %reduce-scatter.2.cloned.1.call-start = ((), (), s32[]{:S(2)}) async-start(), calls=%async_computation.5 | async-start | bytes 13369344 | tf_op jit(solution)/shard_map/reduce_scatter | solution.py:54
  12.0 3.3 copy-start
  12.0 99.7 %copy-start.3 = (f32[2048]{0:T(1024)S(1)}, f32[2048]{0:T(1024)}, u32[]{:S(2)}) copy-start(f32[2048]{0:T(1024)} %param.7) | copy-start | bytes 24580
  210.7 7.5 %copy-start.2 = (bf16[512,2,8,128]{0,3,2,1:T(8,128)(2,1)S(1)}, bf16[512,2,8,128]{0,3,2,1:T(8,128)(2,1)}, u32[]{:S(2)}) copy-start(bf16[512,2,8,128]{0,3,2,1:T(8,128)(2,1)} %copy.12) | copy-start | bytes 6291460
  210.7 7.5 %copy-start.4 = (f32[512,1536]{1,0:T(8,128)S(1)}, f32[512,1536]{1,0:T(8,128)}, u32[]{:S(2)}) copy-start(f32[512,1536]{1,0:T(8,128)} %fusion.14) | copy-start | bytes 9437188
  216.5 1.8 copy-start.6
  225.1 314.5 %all-reduce.2.cloned.1.call-start = ((), (), s32[]{:S(2)}) async-start(), calls=%async_computation.4 | async-start | bytes 4194304 | tf_op jit(solution)/shard_map/psum | solution.py:35
  309.8 8.6 %copy-start.5 = (f32[512,1536]{1,0:T(8,128)S(1)}, f32[512,1536]{1,0:T(8,128)}, u32[]{:S(2)}) copy-start(f32[512,1536]{1,0:T(8,128)} %fusion.14) | copy-start | bytes 9437188
  309.8 8.6 %copy-start.7 = (f32[512,1536]{1,0:T(8,128)S(1)}, f32[512,1536]{1,0:T(8,128)}, u32[]{:S(2)}) copy-start(f32[512,1536]{1,0:T(8,128)} %copy-done.6) | copy-start | bytes 9437188
  309.8 17.2 %slice-start = ((s8[6291456]{0:T(1024)(128)(4,1)}), s8[4194304]{0:T(1024)(128)(4,1)S(1)}, s32[]{:S(2)}) async-start(s8[6291456]{0:T(1024)(128)(4,1)} %bitcast.15), calls=%async_computation.7 | async-start | bytes 8388608
  318.4 8.6 %slice-start.1 = ((s8[6291456]{0:T(1024)(128)(4,1)}), s8[2097152]{0:T(1024)(128)(4,1)S(1)}, s32[]{:S(2)}) async-start(s8[6291456]{0:T(1024)(128)(4,1)} %bitcast.15), calls=%async_computation.8 | async-start | bytes 4194304
  333.7 257.1 %all-gather.11.cloned.1.call-start = ((), (), s32[]{:S(2)}) async-start(), calls=%async_computation.6 | async-start | bytes 2359296 | tf_op jit(solution)/shard_map/all_gather | solution.py:60
Sparse Core Ops, SparseCore 0:
  10.2 101.4 all-gather.8
  113.8 96.8 all-gather.6
  212.9 96.8 all-gather.4
  315.3 200.6 reduce-scatter.1
  518.8 20.7 all-reduce.1
  541.0 28.3 all-gather.10
where the time goes:
time: 601 us
  waiting for transfers between devices  480 us (80%)
  matrix products  44.2 us (7%)
  blocking collectives  43.3 us (7%)
  between operations  14.2 us (2%)
  local copies, waits for them, and re-layouts  10.6 us (2%)
  other arithmetic  8.39 us (1%)
    reduce_scatter x1, waiting for transfers between devices, local(): lax.psum_scatter(0.5 * lax.dot_general(reordered, hidden, contract_rows,...  182 us
    all_gather x1, waiting for transfers between devices, local(): lax.all_gather(gate_weight, 'fs', axis=0, tiled=True)  95.9 us
    all_gather x1, waiting for transfers between devices, local(): lax.all_gather(up_weight, 'fs', axis=0, tiled=True)  91.2 us
    all_gather x1, waiting for transfers between devices, local(): lax.all_gather(down_weight, 'fs', axis=0, tiled=True)  84.5 us
    psum x1, blocking collectives, local(): lax.psum(jnp.sum(normalized_gradient * unit_input, axis=0), ('rep', 'fs'))  43.3 us
    psum x1, waiting for transfers between devices, local(): summed_units = lax.psum(partial_value.astype(jnp.bfloat16), 'tp')  23.6 us
  transfers between devices with their start and end apart: 6, of which 5 were waited for; matrix products, arithmetic and copies ran while one was open for 10% of the time, Pallas kernels for 0%

commit v1 on v0

--- a/solution.py
+++ b/solution.py
@@ -4,6 +4,28 @@
 from jax.sharding import PartitionSpec as P
 
 EPS = 1e-06
+
+
+def in_order(blocks, dim):
+    shape = list(blocks.shape[1:])
+    shape[dim] *= blocks.shape[0]
+    return jnp.moveaxis(blocks, 0, dim).reshape(shape)
+
+
+def grow_blocks(x, axis):
+    size = lax.axis_size(axis)
+    blocks = x[None]
+    for level in range(size.bit_length() - 1):
+        bit = 1 << level
+        other = lax.ppermute(blocks, axis, [(i, i ^ bit) for i in range(size)])
+        both = jnp.stack([blocks, other])
+        upper = lax.axis_index(axis) >> level & 1
+        blocks = jnp.where(upper == 0, both, both[::-1]).reshape(-1, *x.shape)
+    return blocks
+
+
+def collect(x, axis, dim):
+    return in_order(grow_blocks(x, axis), dim)
 
 
 def local(inputs, gain, gate_weight, up_weight, down_weight, cotangent):
@@ -17,7 +39,7 @@
     contract_cols = (((1,), (1,)), ((), ()))
     gate_full, up_full, down_full = (
         lax.all_gather(gate_weight, "fs", axis=0, tiled=True),
-        lax.all_gather(up_weight, "fs", axis=0, tiled=True),
+        collect(up_weight, "fs", 0),
         lax.all_gather(down_weight, "fs", axis=0, tiled=True),
     )
     gate = jnp.dot(normalized_input, gate_full, preferred_element_type=jnp.float32)

time: 601 us -> 656 us (1.092)
  waiting for transfers between devices: 480 us -> 519 us
  other arithmetic: 8.39 us -> 18.8 us
    ppermute x0 -> x3, waiting for transfers between devices: none -> 316 us  [grow_blocks(): other = lax.ppermute(blocks, axis, [(i, i ^ bit) for i in range(size)])]
    all_gather x1, waiting for transfers between devices: 95.9 us -> 0.01 us  [local(): lax.all_gather(gate_weight, 'fs', axis=0, tiled=True)]
    all_gather x1 -> x0, waiting for transfers between devices: 91.2 us -> none  [local(): lax.all_gather(up_weight, 'fs', axis=0, tiled=True)]
    all_gather x1, waiting for transfers between devices: 84.5 us -> 0.02 us  [local(): lax.all_gather(down_weight, 'fs', axis=0, tiled=True)]
    another operation x0 -> x4, other arithmetic: none -> 6.79 us  [grow_blocks(): both = jnp.stack([blocks, other])]
  transfers between devices with their start and end apart: 6 -> 8, of which waited for: 5 -> 5; matrix products, arithmetic and copies ran while one was open for 10% -> 10% of each run, Pallas kernels for 0% -> 0%
where the time goes in v1:
time: 656 us
  waiting for transfers between devices  519 us (79%)
  blocking collectives  43.3 us (7%)
  matrix products  41.6 us (6%)
  other arithmetic  18.8 us (3%)
  between operations  13.9 us (2%)
  local copies, waits for them, and re-layouts  13.1 us (2%)
    ppermute x3, waiting for transfers between devices, grow_blocks(): other = lax.ppermute(blocks, axis, [(i, i ^ bit) for i in range(size)])  316 us
    reduce_scatter x1, waiting for transfers between devices, local(): lax.psum_scatter(0.5 * lax.dot_general(reordered, hidden, contract_rows,...  179 us
    psum x1, blocking collectives, local(): lax.psum(jnp.sum(normalized_gradient * unit_input, axis=0), ('rep', 'fs'))  43.3 us
    psum x1, waiting for transfers between devices, local(): summed_units = lax.psum(partial_value.astype(jnp.bfloat16), 'tp')  23.6 us
  transfers between devices with their start and end apart: 8, of which 5 were waited for; matrix products, arithmetic and copies ran while one was open for 10% of the time, Pallas kernels for 0%

profile of v1, /device:TPU:0, one launch (start us, length us, event | category | flops | bytes accessed | tf_op | source)
XLA Modules:
  0.0 656.0 jit_solution(15803119656773421328)
XLA Ops:
  7.2 0.0 all-gather.6.cloned.1.call-start
  7.2 0.7 all-gather.6.cloned.1.call-update
  7.9 0.0 all-gather.4.cloned.1.call-start
  7.9 3.1 collective-permute-start
  11.0 0.0 all-gather.4.cloned.1.call-update
  11.0 0.0 reduce-scatter.2.cloned.1.call-start
  11.1 24.5 %collective-permute-done = bf16[1,256,1536]{2,1,0:T(8,128)(2,1)S(1)} collective-permute-done((bf16[1,256,1536]{2,1,0:T(8,128)(2,1)}, bf16[1,256,1536]{2,1,0:T(8,128)(2,1)S(1)}, u32[]{:S(2)}, u32[]{:S(2)}) %collective-permute-start) | collective-permute-done | bytes 786464 | tf_op jit(solution)/shard_map/ppermute | solution.py:20
  35.6 1.3 pad_maximum_fusion.2
  36.9 0.4 fusion.15
  37.3 1.5 collective-permute-start.1
  38.7 85.5 %collective-permute-done.1 = bf16[2,256,1536]{2,1,0:T(8,128)(2,1)} collective-permute-done((bf16[2,256,1536]{2,1,0:T(8,128)(2,1)S(1)}, bf16[2,256,1536]{2,1,0:T(8,128)(2,1)}, u32[]{:S(2)}, u32[]{:S(2)}) %collective-permute-start.1) | collective-permute-done | bytes 1572896 | tf_op jit(solution)/shard_map/ppermute | solution.py:20
  124.2 1.7 pad_maximum_fusion.1
  126.0 0.0 copy-start.1
  126.0 2.3 reverse_select_fusion.1
  128.2 0.9 collective-permute-start.2
  129.2 0.0 copy-done.1
  129.2 2.5 copy.11
  131.7 0.0 copy-start
  131.7 3.3 copy.12
  134.9 0.0 copy-done
  134.9 0.5 fusion.9
  135.4 205.8 %collective-permute-done.2 = bf16[4,256,1536]{2,1,0:T(8,128)(2,1)} collective-permute-done((bf16[4,256,1536]{2,1,0:T(8,128)(2,1)}, bf16[4,256,1536]{2,1,0:T(8,128)(2,1)}, u32[]{:S(2)}, u32[]{:S(2)}) %collective-permute-start.2) | collective-permute-done | bytes 3145760 | tf_op jit(solution)/shard_map/ppermute | solution.py:20
  341.2 3.4 pad_maximum_fusion
  344.6 0.0 copy-start.4
  344.6 1.3 reverse_select_fusion
  346.0 0.0 copy-start.2
  346.0 2.7 copy-done.2
  348.7 0.0 copy-done.4
  348.7 5.2 fusion.18
  353.8 0.0 all-gather.6.cloned.1.call-done
  353.9 0.0 copy-start.3
  353.9 0.0 copy-start.5
  353.9 5.8 fusion.16
  359.6 0.0 copy-start.7
  359.6 1.6 copy-done.7
  361.2 0.0 copy-done.3
  361.2 0.0 copy-done.5
  361.2 7.0 %multiply_bitcast_fusion = f32[2048,1536]{0,1:T(8,128)} fusion(bf16[512,2048]{0,1:T(8,128)(2,1)S(1)} %bitcast.30, f32[512,1536]{1,0:T(8,128)S(1)} %copy-done.5, f32[512,1536]{1,0:T(8,128)S(1)} %fusion.16), kind=kOutput, calls=%fused_computation | convolution fusion | flops 3229089792 | bytes 20971520 | tf_op jit(solution)/shard_map/dot_general | solution.py:77
  368.2 0.0 reduce-scatter.2.cloned.1.call-update
  368.2 0.2 all-reduce.2.cloned.1.call-start
  368.5 0.0 all-gather.4.cloned.1.call-done
  368.5 0.0 copy-start.6
  368.5 0.0 copy-start.8
  368.5 0.0 slice-start
  368.5 8.6 %convolution_multiply_fusion = f32[512,1536]{1,0:T(8,128)} fusion(bf16[512,2048]{1,0:T(8,128)(2,1)} %param.11, bf16[2048,1536]{1,0:T(8,128)(2,1)} %all-gather.4.cloned.1.call-done), kind=kOutput, calls=%fused_computation.20 | convolution fusion | flops 3222011904 | bytes 11534336 | tf_op jit(solution)/shard_map/dot_general | solution.py:47
  377.1 0.0 copy-done.6
  377.1 0.0 copy-done.8
  377.1 0.0 slice-start.1
  377.1 8.5 %fusion.12 = f32[512,2048]{1,0:T(8,128)S(1)} fusion(bf16[2048,1536]{1,0:T(8,128)(2,1)} %all-gather.6.cloned.1.call-done, f32[512,1536]{1,0:T(8,128)S(1)} %copy-done.8, f32[512,1536]{1,0:T(8,128)} %convolution_multiply_fusion, f32[512,1536]{1,0:T(8,128)S(1)} %copy-done.6), kind=kOutput, calls=%fused_computation.28 | convolution fusion | flops 3229089792 | bytes 19922944 | tf_op jit(solution)/shard_map/dot_general | solution.py:54
  385.6 0.0 slice-done
  385.7 0.0 slice-done.1
  385.7 6.6 %add_convert_fusion = bf16[512,2048]{1,0:T(8,128)(2,1)} fusion(f32[512,2048]{1,0:T(8,128)S(1)} %fusion.12, bf16[2048,1536]{1,0:T(8,128)(2,1)S(1)} %bitcast.29, f32[512,1536]{1,0:T(8,128)} %convolution_multiply_fusion, f32[512,1536]{1,0:T(8,128)S(1)} %copy-done.8), kind=kOutput, calls=%fused_computation.19 | convolution fusion | flops 3228041216 | bytes 18874368 | tf_op jit(solution)/shard_map/dot_general | solution.py:56
  392.3 0.0 all-reduce.2.cloned.1.call-update
  392.3 0.0 all-gather.8.cloned.1.call-start
  392.4 179.2 %reduce-scatter.2.cloned.1.call-done = f32[128,1536]{0,1:T(8,128)} async-done(((f32[2048,1536]{0,1:T(8,128)}), f32[128,1536]{0,1:T(8,128)}) %reduce-scatter.2.cloned.1.call-update) | async-done | bytes 786448 | tf_op jit(solution)/shard_map/reduce_scatter | solution.py:76
  571.6 0.0 all-gather.8.cloned.1.call-update
  571.6 23.6 %all-reduce.2.cloned.1.call-done = bf16[512,2048]{1,0:T(8,128)(2,1)} async-done(((bf16[512,2048]{1,0:T(8,128)(2,1)}), bf16[512,2048]{1,0:T(8,128)(2,1)}) %all-reduce.2.cloned.1.call-update) | async-done | bytes 2097168 | tf_op jit(solution)/shard_map/psum | solution.py:57
  595.2 2.9 fusion.10
  598.1 43.3 %psum.15 = f32[2048]{0:T(1024)} all-reduce(f32[2048]{0:T(1024)S(1)} %get-tuple-element.12), channel_id=1, replica_groups=mesh['rep'=2,'fs'=8,'tp'=2] {'rep','fs'}, use_global_device_ids=true, to_apply=%region_4.5 | all-reduce | flops 2048 | bytes 16384 | tf_op jit(solution)/shard_map/psum | solution.py:59
  641.4 5.0 fusion.6
  646.4 0.0 all-gather.8.cloned.1.call-done
  646.4 3.0 copy.13
  (3 shorter events, 0.0 us)
Async XLA Ops:
  7.2 346.7 %all-gather.6.cloned.1.call-start = ((), (), s32[]{:S(2)}) async-start(), calls=%async_computation.2 | async-start | bytes 7077888 | tf_op jit(solution)/shard_map/all_gather | solution.py:41
  7.9 360.6 %all-gather.4.cloned.1.call-start = ((), (), s32[]{:S(2)}) async-start(), calls=%async_computation.1 | async-start | bytes 7077888 | tf_op jit(solution)/shard_map/all_gather | solution.py:43
  7.9 27.7 %collective-permute-start = (bf16[1,256,1536]{2,1,0:T(8,128)(2,1)}, bf16[1,256,1536]{2,1,0:T(8,128)(2,1)S(1)}, u32[]{:S(2)}, u32[]{:S(2)}) collective-permute-start(bf16[1,256,1536]{2,1,0:T(8,128)(2,1)} %bitcast.31), channel_id=1, source_target_pairs={{0,2},{2,0},{4,6},{6,4},{8,10},{10,8},{12,14},{14,12},{1,3},{3,1},... | collective-permute-start | bytes 2359304 | tf_op jit(solution)/shard_map/ppermute | solution.py:20
  11.0 560.5 %reduce-scatter.2.cloned.1.call-start = ((), (), s32[]{:S(2)}) async-start(), calls=%async_computation.4 | async-start | bytes 13369344 | tf_op jit(solution)/shard_map/reduce_scatter | solution.py:76
  37.3 87.0 %collective-permute-start.1 = (bf16[2,256,1536]{2,1,0:T(8,128)(2,1)S(1)}, bf16[2,256,1536]{2,1,0:T(8,128)(2,1)}, u32[]{:S(2)}, u32[]{:S(2)}) collective-permute-start(bf16[2,256,1536]{2,1,0:T(8,128)(2,1)S(1)} %get-tuple-element.15), channel_id=1, source_target_pairs={{0,4},{2,6},{4,0},{6,2},{8,12},{10,14},{12,8},{14,10},{1,5},{3,7},... | collective-permute-start | bytes 4718600 | tf_op jit(solution)/shard_map/ppermute | solution.py:20
  126.0 3.2 copy-start.1
  128.2 212.9 %collective-permute-start.2 = (bf16[4,256,1536]{2,1,0:T(8,128)(2,1)}, bf16[4,256,1536]{2,1,0:T(8,128)(2,1)}, u32[]{:S(2)}, u32[]{:S(2)}) collective-permute-start(bf16[4,256,1536]{2,1,0:T(8,128)(2,1)} %bitcast.7), channel_id=1, source_target_pairs={{0,8},{2,10},{4,12},{6,14},{8,0},{10,2},{12,4},{14,6},{1,9},{3,11}... | collective-permute-start | bytes 9437192 | tf_op jit(solution)/shard_map/ppermute | solution.py:20
  131.7 3.3 copy-start
  344.6 4.1 copy-start.4
  346.0 2.7 copy-start.2
  353.9 7.4 %copy-start.3 = (bf16[512,2,8,128]{0,3,2,1:T(8,128)(2,1)S(1)}, bf16[512,2,8,128]{0,3,2,1:T(8,128)(2,1)}, u32[]{:S(2)}) copy-start(bf16[512,2,8,128]{0,3,2,1:T(8,128)(2,1)} %copy.12) | copy-start | bytes 6291460
  353.9 7.4 %copy-start.5 = (f32[512,1536]{1,0:T(8,128)S(1)}, f32[512,1536]{1,0:T(8,128)}, u32[]{:S(2)}) copy-start(f32[512,1536]{1,0:T(8,128)} %fusion.18) | copy-start | bytes 9437188
  359.6 1.6 copy-start.7
  368.2 227.0 %all-reduce.2.cloned.1.call-start = ((), (), s32[]{:S(2)}) async-start(), calls=%async_computation.3 | async-start | bytes 4194304 | tf_op jit(solution)/shard_map/psum | solution.py:57
  368.5 8.6 %copy-start.6 = (f32[512,1536]{1,0:T(8,128)S(1)}, f32[512,1536]{1,0:T(8,128)}, u32[]{:S(2)}) copy-start(f32[512,1536]{1,0:T(8,128)} %fusion.18) | copy-start | bytes 9437188
  368.5 8.6 %copy-start.8 = (f32[512,1536]{1,0:T(8,128)S(1)}, f32[512,1536]{1,0:T(8,128)}, u32[]{:S(2)}) copy-start(f32[512,1536]{1,0:T(8,128)} %copy-done.7) | copy-start | bytes 9437188
  368.5 17.2 %slice-start = ((s8[6291456]{0:T(1024)(128)(4,1)}), s8[4194304]{0:T(1024)(128)(4,1)S(1)}, s32[]{:S(2)}) async-start(s8[6291456]{0:T(1024)(128)(4,1)} %bitcast.27), calls=%async_computation.6 | async-start | bytes 8388608
  377.1 8.6 %slice-start.1 = ((s8[6291456]{0:T(1024)(128)(4,1)}), s8[2097152]{0:T(1024)(128)(4,1)S(1)}, s32[]{:S(2)}) async-start(s8[6291456]{0:T(1024)(128)(4,1)} %bitcast.27), calls=%async_computation.7 | async-start | bytes 4194304
  392.3 254.1 %all-gather.8.cloned.1.call-start = ((), (), s32[]{:S(2)}) async-start(), calls=%async_computation.5 | async-start | bytes 2359296 | tf_op jit(solution)/shard_map/all_gather | solution.py:82
Sparse Core Ops, SparseCore 0:
  10.2 130.0 all-gather.5
  142.4 183.2 all-gather.3
  368.3 203.1 reduce-scatter.1
  574.3 20.7 all-reduce.1
  596.6 28.3 all-gather.7
